TPU v7x, 32 devices: a whole 2x2x4 slice. The times are simulated.
32 devices in a mesh: fs: 8 (over z, x), tp: 4 (over y, core).
Axes of the slice: x: 2, y: 2, z: 4, core: 2. Of those that a mesh axis runs over, the one named last changes fastest.
Arguments:
- tokens: bfloat16 [4096, 2048], P(('fs', 'tp')), may hold values from -6 to 6
- norm_gain: float32 [2048], P('fs'), may hold values from 0.1 to 1.9
- gate_proj: float32 [32, 2048, 512], P(None, 'fs', 'tp'), may hold values from -0.125 to 0.125
- up_proj: float32 [32, 2048, 512], P(None, 'fs', 'tp'), may hold values from -0.125 to 0.125
- down_proj: float32 [32, 512, 2048], P(None, 'fs', 'tp'), may hold values from -0.25 to 0.25
- expert_ids: int32 [4096, 2], P(('fs', 'tp')), may hold values from 0 to 31, as said below
- route_weight: float32 [4096, 2], P(('fs', 'tp')), may hold values from 0.05 to 1
Outputs:
- mixed: bfloat16 [4096, 2048], P(('fs', 'tp'))
- new_gate: bfloat16 [32, 2048, 512], P(('fs', 'tp'))
- new_up: bfloat16 [32, 2048, 512], P(('fs', 'tp'))
- new_down: bfloat16 [32, 512, 2048], P(('fs', 'tp'))
Inputs may be any that keep to these rules, and one draw needn't show every extreme that they name: `expert_ids`: the two experts of a row differ and lie in one group of 4 consecutive experts. In each aligned block of 128 rows (the rows of one device) every group is named by exactly 16 rows, no expert by more than 16 rows, and one expert, the same in all blocks, by exactly 16 rows.
All inputs are finite; a program needn't handle non-finite values.
Results may differ from a plain program's by a relative error of at most 0.0087.
Values may be sent and summed in bfloat16 or wider, within the bound.
A program may use at most 128 MiB of HBM per device.

v0:
```python
import functools

import jax
import jax.numpy as jnp
from jax import lax
from jax.experimental import pallas as pl
from jax.experimental.pallas import tpu as pltpu
from jax.sharding import PartitionSpec as P

norm_eps = 1e-06
group_size = 4
extra_lanes = 128
MESH = pl.DeviceIdType.MESH


def shards_plain(tokens, norm_gain, gate_proj, up_proj, down_proj, expert_ids, route_weight):
    row_scale = norm_gain[None, :, None]
    gate_low = (gate_proj * row_scale).astype(jnp.bfloat16)
    up_low = (up_proj * row_scale).astype(jnp.bfloat16)
    down_low = down_proj.astype(jnp.bfloat16)
    width_fs = lax.axis_size("fs")
    width_tp = lax.axis_size("tp")

    def expand(matrix):
        return matrix.reshape((matrix.shape[0], 1) + matrix.shape[1:])

    def assemble(pieces):
        row_count, col_count = (pieces.shape[2], pieces.shape[3])
        tiled = pieces.reshape(width_fs, width_tp, row_count, col_count).transpose(0, 2, 1, 3)
        return tiled.reshape(1, width_fs * row_count, width_tp * col_count)

    arrived = (
        lax.all_to_all(expand(gate_low), ("fs", "tp"), split_axis=0, concat_axis=1, tiled=True),
        lax.all_to_all(expand(up_low), ("fs", "tp"), split_axis=0, concat_axis=1, tiled=True),
        lax.all_to_all(expand(down_low), ("fs", "tp"), split_axis=0, concat_axis=1, tiled=True),
    )
    new_gate, new_up, new_down = (assemble(arrived[0]), assemble(arrived[1]), assemble(arrived[2]))
    tok_count, width = tokens.shape
    experts = gate_proj.shape[0]
    slot_cap = 4 * tok_count // experts
    widened = tokens.astype(jnp.float32)
    normed = (
        widened * lax.rsqrt(jnp.mean(widened * widened, axis=-1, keepdims=True) + norm_eps)
    ).astype(jnp.bfloat16)
    flat_ids = expert_ids.reshape(-1)
    onehot = (flat_ids[:, None] == jnp.arange(experts, dtype=jnp.int32)[None, :]).astype(jnp.int32)
    slot_rank = jnp.sum(jnp.cumsum(onehot, axis=0) * onehot, axis=1) - 1
    slot_index = flat_ids * slot_cap + slot_rank
    source = (
        jnp.zeros((experts * slot_cap,), jnp.int32)
        .at[slot_index]
        .set(jnp.arange(2 * tok_count, dtype=jnp.int32) // 2 + 1)
    )
    filled = source > 0
    outgoing = jnp.where(
        filled[:, None], normed[jnp.maximum(source - 1, 0)], jnp.zeros((), jnp.bfloat16)
    )
    outgoing = outgoing.reshape(experts, slot_cap, width)
    arrived_rows = lax.all_to_all(outgoing, ("fs", "tp"), split_axis=0, concat_axis=0, tiled=True)
    flat_rows = arrived_rows.reshape(-1, width)
    gate_act = jnp.dot(flat_rows, new_gate[0], preferred_element_type=jnp.float32)
    up_act = jnp.dot(flat_rows, new_up[0], preferred_element_type=jnp.float32)
    hidden = (jax.nn.silu(gate_act) * up_act).astype(jnp.bfloat16)
    results = jnp.dot(hidden, new_down[0], preferred_element_type=jnp.float32).astype(jnp.bfloat16)
    returned = lax.all_to_all(
        results.reshape(arrived_rows.shape), ("fs", "tp"), split_axis=0, concat_axis=0, tiled=True
    )
    picked = returned.reshape(experts * slot_cap, width)[slot_index].reshape(tok_count, 2, width)
    mixed = jnp.sum(route_weight[:, :, None] * picked.astype(jnp.float32), axis=1).astype(
        jnp.bfloat16
    )
    return (mixed, new_gate, new_up, new_down)


def fused_kernel(
    n_fs, n_tp,
    x_ref, ids_ref, rw_ref, gain_ref, gate_in, up_in, down_in,
    gate_out, up_out, down_out, perm, fin_rx,
    gate_st, up_st, down_st, gate_tx, up_tx, down_tx, gate_w, up_w, down_w,
    tok_tx, rows, hidden, own, part_tx, part_rx, sum_tx, sum_rx, fin_tx,
    ld_sem, w_send, w_recv, tok_send, tok_recv, ex_send, ex_recv, red_send, red_recv,
    y_send, y_recv, fin_send, fin_recv, out_sem,
):
    f32, bf16 = jnp.float32, jnp.bfloat16
    fs, tp = lax.axis_index("fs"), lax.axis_index("tp")
    core = lax.rem(tp, 2)
    pair = tp // 2
    partner = tp + 1 - 2 * core
    across = lax.rem(tp + 2, n_tp)
    n_dev = n_fs * n_tp
    toks, width = x_ref.shape
    per = toks // n_fs
    srcs = (gate_in, up_in, down_in)
    stages = (gate_st, up_st, down_st)
    txs = (gate_tx, up_tx, down_tx)
    lands = (gate_w, up_w, down_w)
    outs = (gate_out, up_out, down_out)

    barrier = pltpu.get_barrier_semaphore()

    @pl.loop(1, n_dev)
    def _(k):
        dev = lax.rem(fs * n_tp + tp + k, n_dev)
        pl.semaphore_signal(
            barrier, inc=1, device_id=(dev // n_tp, lax.rem(dev, n_tp)), device_id_type=MESH
        )

    quarter = n_fs // 4
    layer, col = fs // quarter, lax.rem(fs, quarter)
    half = layer // 2
    inner_far, outer_far, mate = 2 - half, 3 - 3 * half, 4 * half + 1 - layer

    def targets(layers):
        return [
            (at * quarter + lax.rem(col + 1 + i, quarter), at is layer and i == quarter - 1)
            for i in range(quarter)
            for at in layers
        ]

    orders = ((outer_far, inner_far), (mate, layer))
    plan = [
        (ms, goal) for at in orders for ms in ((0, 1), (2,)) for goal in targets(at)
    ]

    def load(m, tgt):
        at = pl.ds(tgt * n_tp, n_tp)
        return pltpu.make_async_copy(srcs[m].at[at], stages[m].at[at], ld_sem.at[m, tgt])

    for ms, (tgt, _) in plan:
        for m in ms:
            load(m, tgt).start()

    pl.semaphore_wait(barrier, n_dev - 1)

    lane = lax.broadcasted_iota(jnp.int32, (toks, extra_lanes), 1).astype(f32)
    lane_pick = jnp.where(lane < group_size, lane, lane - group_size)
    def as_columns(flat):
        spread_rows = jnp.concatenate([flat] * (8 // flat.shape[0]), axis=0)
        return jnp.transpose(spread_rows)

    def span(i):
        return pl.ds(pl.multiple_of(i * per, per), per)

    def spread(tx, land, send_sem, recv_sem):
        @pl.loop(1, n_fs)
        def _(j):
            tgt = lax.rem(fs + j, n_fs)
            pltpu.make_async_remote_copy(
                src_ref=tx.at[span(tgt)], dst_ref=land.at[span(fs)],
                send_sem=send_sem, recv_sem=recv_sem,
                device_id=(tgt, tp), device_id_type=MESH,
            ).start()

        pltpu.make_async_copy(tx.at[span(fs)], land.at[span(fs)], recv_sem).start()

    def all_sent(tx, sem, count):
        part = tx.at[pl.ds(0, count)]
        pltpu.make_async_copy(part, part, sem).wait()

    def all_here(land, sem):
        pltpu.make_async_copy(land, land, sem).wait()


    gain = jnp.broadcast_to(as_columns(gain_ref[...])[:, 0:1], gate_in.shape[1:])

    def cast(ms, tgt):
        for m in ms:
            load(m, tgt).wait()

            @pl.loop(0, n_tp)
            def _(t):
                block = stages[m][tgt * n_tp + t]
                if m < 2:
                    block = block * gain
                txs[m][tgt * n_tp + t] = block.astype(bf16)

    def block_at(m):
        r, c = srcs[m].shape[1:]
        return lands[m].at[pl.ds(pl.multiple_of(fs * r, r), r), pl.ds(pl.multiple_of(tp * c, c), c)]

    def send(ms, tgt, first):
        for t in range(first, n_tp):
            to = lax.rem(tp + t, n_tp)
            for m in ms:
                pltpu.make_async_remote_copy(
                    src_ref=txs[m].at[tgt * n_tp + to], dst_ref=block_at(m),
                    send_sem=w_send.at[m], recv_sem=w_recv.at[m],
                    device_id=(tgt, to), device_id_type=MESH,
                ).start()

    def step_plan(first, last):
        for k in range(first, last):
            if k < len(plan):
                cast(plan[k][0], plan[k][1][0])
            if k > 0:
                ms, (tgt, same) = plan[k - 1]
                send(ms, tgt, 1 if same else 0)
                if same:
                    for m in ms:
                        pltpu.make_async_copy(
                            txs[m].at[fs * n_tp + tp], block_at(m), w_recv.at[m]
                        ).start()

    step_plan(0, 3)

    x = x_ref[...].astype(f32)
    scale = lax.rsqrt(jnp.mean(x * x, axis=-1, keepdims=True) + norm_eps)
    normed = (x * scale).astype(bf16)
    idf = as_columns(ids_ref[...].astype(f32))
    grp = jnp.floor((idf + 0.5) * (1.0 / group_size))
    slot = lax.broadcasted_iota(jnp.int32, (toks, toks), 1).astype(f32)
    tok = lax.broadcasted_iota(jnp.int32, (toks, toks), 0).astype(f32)
    slot_grp = jnp.floor((slot + 0.5) * (1.0 / per))
    named = (grp[:, 0:1] == slot_grp).astype(f32)
    before = (slot < tok).astype(f32)
    rank = jnp.dot(before.astype(bf16), named.astype(bf16), preferred_element_type=f32)
    place = jnp.where(rank == slot - slot_grp * per, named, 0.0).astype(bf16)
    perm[...] = place
    local = idf - grp * group_size
    rw = as_columns(rw_ref[...])
    wv = jnp.where(local[:, 0:1] == lane_pick, rw[:, 0:1], 0.0) + jnp.where(
        local[:, 1:2] == lane_pick, rw[:, 1:2], 0.0
    )
    high = wv.astype(bf16)
    low = (wv - high.astype(f32)).astype(bf16)
    aug = jnp.where(
        lane < group_size,
        high.astype(f32),
        jnp.where(lane < 2 * group_size, low.astype(f32), 0.0),
    ).astype(bf16)
    by_slot = (((0,), (0,)), ((), ()))
    tok_tx[:, 0:width] = lax.dot_general(
        place, normed, by_slot, preferred_element_type=f32
    ).astype(bf16)
    tok_tx[:, width:] = lax.dot_general(
        place, aug, by_slot, preferred_element_type=f32
    ).astype(bf16)
    spread(tok_tx, rows.at[tp], tok_send, tok_recv)

    step_plan(3, len(plan) + 1)

    def swap(src, dst, to, send_sem, recv_sem):
        return pltpu.make_async_remote_copy(
            src_ref=src, dst_ref=dst, send_sem=send_sem, recv_sem=recv_sem,
            device_id=(fs, to), device_id_type=MESH,
        )

    all_here(rows.at[tp], tok_recv)
    cross = swap(rows.at[tp], rows.at[tp], across, ex_send.at[0], ex_recv.at[0])
    cross.start()
    near = swap(rows.at[tp], rows.at[tp], partner, ex_send.at[1], ex_recv.at[1])
    near.start()
    cross.wait()
    far = swap(rows.at[across], rows.at[across], partner, ex_send.at[2], ex_recv.at[2])
    far.start()
    near.wait()
    far.wait()

    for m in (0, 1):
        all_here(lands[m], w_recv.at[m])
        pltpu.make_async_copy(lands[m], outs[m], out_sem.at[m]).start()

    @pl.loop(0, n_tp)
    def _(q):
        block = rows[q, :, 0:width]
        g = jnp.dot(block, gate_w[...], preferred_element_type=f32)
        u = jnp.dot(block, up_w[...], preferred_element_type=f32)
        hidden[q] = (g / (1.0 + jnp.exp(-g)) * u).astype(bf16)

    all_here(down_w, w_recv.at[2])
    pltpu.make_async_copy(down_w, down_out, out_sem.at[2]).start()

    tpf = tp.astype(f32)

    def partial(q):
        w = jnp.sum(
            jnp.where(lane_pick == tpf, rows[q, :, width:].astype(f32), 0.0),
            axis=-1, keepdims=True,
        )
        return jnp.dot(hidden[q], down_w[...], preferred_element_type=f32) * w

    def reduce_near(i, p):
        return swap(part_tx.at[i], part_rx.at[i], partner, red_send.at[i], red_recv.at[i])

    def give(i, side):
        part_tx[i] = partial(side * 2 + 1 - core).astype(bf16)
        reduce_near(i, partner).start()
        own[i] = partial(side * 2 + core)
        reduce_near(i, partner).wait()
        own[i] = own[i] + part_rx[i].astype(f32)

    pieces = 4
    step = n_fs // pieces

    def piece(p):
        return lax.rem(half * 2 + 2 + p, pieces)

    def piece_rows(p):
        return pl.ds(pl.multiple_of(piece(p) * step * per, step * per), step * per)

    def over(p):
        at = piece_rows(p)
        return swap(sum_tx.at[at], sum_rx.at[at], across, y_send.at[p], y_recv.at[p])

    give(0, 1 - pair)
    for p in range(pieces):
        at = piece_rows(p)
        sum_tx[at] = own[0, at].astype(bf16)
    for p in range(pieces):
        over(p).start()
    give(1, pair)

    def give_back(p):
        for i in range(step):
            to = piece(p) * step + i

            @pl.when(to != fs)
            def _():
                pltpu.make_async_remote_copy(
                    src_ref=fin_tx.at[span(to)], dst_ref=fin_rx.at[span(fs)],
                    send_sem=fin_send, recv_sem=fin_recv,
                    device_id=(to, tp), device_id_type=MESH,
                ).start()

            @pl.when(to == fs)
            def _():
                pltpu.make_async_copy(
                    fin_tx.at[span(fs)], fin_rx.at[span(fs)], fin_recv
                ).start()

    for p in range(pieces):
        over(p).wait()
        at = piece_rows(p)
        fin_tx[at] = (own[1, at] + sum_rx[at].astype(f32)).astype(bf16)
        give_back(p)
    for m in range(3):
        all_sent(txs[m], w_send.at[m], n_dev - 1)
        pltpu.make_async_copy(lands[m], outs[m], out_sem.at[m]).wait()
    all_sent(tok_tx, tok_send, toks - per)
    all_sent(fin_tx, fin_send, toks - per)
    all_here(fin_rx, fin_recv)


def write_kernel(perm, fin_rx, gate, up, down, mixed_ref, gate_out, up_out, down_out, gate_v, up_v, down_v, sem_in, sem_out):
    chunks = sem_in.shape[1]
    moves = ((gate, gate_v, gate_out), (up, up_v, up_out), (down, down_v, down_out))

    def cut(ref, i):
        size = ref.shape[0] // chunks
        return ref.at[pl.ds(i * size, size)]

    def take(m, i):
        return pltpu.make_async_copy(cut(moves[m][0], i), cut(moves[m][1], i), sem_in.at[m, i])

    def put(m, i):
        return pltpu.make_async_copy(cut(moves[m][1], i), cut(moves[m][2], i), sem_out.at[m, i])

    every = [(m, i) for m in range(3) for i in range(chunks)]
    for m, i in every:
        take(m, i).start()
    mixed_ref[...] = jnp.dot(
        perm[...], fin_rx[...], preferred_element_type=jnp.float32
    ).astype(jnp.bfloat16)
    for m, i in every:
        take(m, i).wait()
        put(m, i).start()
    for m, i in every:
        put(m, i).wait()


def shards_fused(n_fs, n_tp, tokens, norm_gain, gate_proj, up_proj, down_proj, expert_ids, route_weight):
    f32, bf16 = jnp.float32, jnp.bfloat16
    n_dev = n_fs * n_tp
    toks, width = tokens.shape
    _, gr, gc = gate_proj.shape
    _, dr, dc = down_proj.shape
    inner = gc * n_tp
    wide = width + extra_lanes
    vmem = pl.BlockSpec(memory_space=pltpu.VMEM)
    anywhere = pl.BlockSpec(memory_space=pl.ANY)
    dma = pltpu.SemaphoreType.DMA
    new_gate, new_up, new_down, perm, returned = pl.pallas_call(
        functools.partial(fused_kernel, n_fs, n_tp),
        out_shape=(
            jax.ShapeDtypeStruct((width, inner), bf16),
            jax.ShapeDtypeStruct((width, inner), bf16),
            jax.ShapeDtypeStruct((inner, width), bf16),
            jax.ShapeDtypeStruct((toks, toks), bf16),
            jax.ShapeDtypeStruct((toks, width), bf16),
        ),
        in_specs=[vmem] * 4 + [anywhere] * 3,
        out_specs=(anywhere, anywhere, anywhere, vmem, vmem),
        scratch_shapes=[
            pltpu.VMEM((n_dev, gr, gc), f32),
            pltpu.VMEM((n_dev, gr, gc), f32),
            pltpu.VMEM((n_dev, dr, dc), f32),
            pltpu.VMEM((n_dev, gr, gc), bf16),
            pltpu.VMEM((n_dev, gr, gc), bf16),
            pltpu.VMEM((n_dev, dr, dc), bf16),
            pltpu.VMEM((width, inner), bf16),
            pltpu.VMEM((width, inner), bf16),
            pltpu.VMEM((inner, width), bf16),
            pltpu.VMEM((toks, wide), bf16),
            pltpu.VMEM((n_tp, toks, wide), bf16),
            pltpu.VMEM((n_tp, toks, inner), bf16),
            pltpu.VMEM((2, toks, width), f32),
            pltpu.VMEM((2, toks, width), bf16),
            pltpu.VMEM((2, toks, width), bf16),
            pltpu.VMEM((toks, width), bf16),
            pltpu.VMEM((toks, width), bf16),
            pltpu.VMEM((toks, width), bf16),
            dma((3, n_fs)), dma((3,)), dma((3,)), dma, dma, dma((3,)), dma((3,)),
            dma((2,)), dma((2,)), dma((4,)), dma((4,)), dma, dma, dma((3,)),
        ],
        compiler_params=pltpu.CompilerParams(
            collective_id=0, has_side_effects=True, vmem_limit_bytes=60 * 1024 * 1024
        ),
    )(tokens, expert_ids.T, route_weight.T, norm_gain[None, :], gate_proj, up_proj, down_proj)
    mixed, new_gate, new_up, new_down = pl.pallas_call(
        write_kernel,
        out_shape=(
            jax.ShapeDtypeStruct((toks, width), bf16),
            jax.ShapeDtypeStruct((width, inner), bf16),
            jax.ShapeDtypeStruct((width, inner), bf16),
            jax.ShapeDtypeStruct((inner, width), bf16),
        ),
        in_specs=[vmem] * 2 + [anywhere] * 3,
        out_specs=(vmem, anywhere, anywhere, anywhere),
        scratch_shapes=[
            pltpu.VMEM((width, inner), bf16),
            pltpu.VMEM((width, inner), bf16),
            pltpu.VMEM((inner, width), bf16),
            dma((3, 4)), dma((3, 4)),
        ],
    )(perm, returned, new_gate, new_up, new_down)
    return mixed, new_gate[None], new_up[None], new_down[None]


def shards(n_fs, n_tp, *args):
    tokens, _, gate_proj, _, down_proj = args[:5]
    toks, experts = tokens.shape[0], gate_proj.shape[0]
    whole_tiles = (
        n_tp == group_size
        and experts == n_fs * n_tp
        and toks % (16 * n_fs) == 0
        and n_fs % 4 == 0
        and gate_proj.shape[2] % 128 == 0
        and down_proj.shape[2] % 128 == 0
        and gate_proj.shape[1] % 16 == 0
        and down_proj.shape[1] % 16 == 0
    )
    if whole_tiles:
        return shards_fused(n_fs, n_tp, *args)
    return shards_plain(*args)


def solution(mesh):
    in_specs = (
        P(("fs", "tp"), None),
        P("fs"),
        P(None, "fs", "tp"),
        P(None, "fs", "tp"),
        P(None, "fs", "tp"),
        P(("fs", "tp"), None),
        P(("fs", "tp"), None),
    )
    out_specs = (
        P(("fs", "tp"), None),
        P(("fs", "tp"), None, None),
        P(("fs", "tp"), None, None),
        P(("fs", "tp"), None, None),
    )
    body = functools.partial(shards, mesh.shape["fs"], mesh.shape["tp"])
    return jax.shard_map(body, mesh=mesh, in_specs=in_specs, out_specs=out_specs, check_vma=False)
```

profile of v0, /device:TPU:0, one launch (start us, length us, event | category | flops | bytes accessed | tf_op | source)
XLA Modules:
  0.0 188.4 jit_solution(14440355442606263274)
XLA Ops:
  0.6 180.4 %shard_map.102 = (bf16[2048,512]{1,0:T(8,128)(2,1)}, bf16[2048,512]{1,0:T(8,128)(2,1)}, bf16[512,2048]{1,0:T(8,128)(2,1)}, bf16[128,128]{1,0:T(8,128)(2,1)}, bf16[128,2048]{1,0:T(8,128)(2,1)}) custom-call(bf16[128,2048]{1,0:T(8,128)(2,1)} %x_ref.1, s32[2,128]{1,0:T(2,128)} %bitcast.6, f32[2,128]{1,0:T(2,128)} %bitcast.7, f32[1,256]{1,0:T(1,128)} %bitcast.8, ...), custom_call_target="tpu_custom_call" | custom-call | tf_op jit(solution)/shard_map/pallas_call | solution.py:382
  181.1 7.3 %shard_map.103 = (bf16[128,2048]{1,0:T(8,128)(2,1)}, bf16[2048,512]{1,0:T(8,128)(2,1)}, bf16[2048,512]{1,0:T(8,128)(2,1)}, bf16[512,2048]{1,0:T(8,128)(2,1)}) custom-call(bf16[128,128]{1,0:T(8,128)(2,1)} %get-tuple-element.13.perm, bf16[128,2048]{1,0:T(8,128)(2,1)} %get-tuple-element.14.fin_rx, bf16[2048,512]{1,0:T(8,128)(2,1)} %get-tuple-element.15.gate, ...), custom_call_target="tpu_custom_call" | custom-call | tf_op jit(solution)/shard_map/pallas_call | solution.py:419
where the time goes:
time: 189 us; the launch traced here: 188 us
  Pallas kernels  188 us (99%)
    pallas_call x1, Pallas kernels, shards_fused(): pl.pallas_call(functools.partial(fused_kernel, n_fs, n_tp), out_shape=(ja...  180 us
    pallas_call x1, Pallas kernels, shards_fused(): pl.pallas_call(write_kernel, out_shape=(jax.ShapeDtypeStruct((toks, width...  7.32 us

commit v1 on v0

--- a/solution.py
+++ b/solution.py
@@ -74,12 +74,13 @@
 
 def fused_kernel(
     n_fs, n_tp,
-    x_ref, ids_ref, rw_ref, gain_ref, gate_in, up_in, down_in,
-    gate_out, up_out, down_out, perm, fin_rx,
-    gate_st, up_st, down_st, gate_tx, up_tx, down_tx, gate_w, up_w, down_w,
+    x_in, ids_in, rw_in, gain_in, gate_in, up_in, down_in,
+    gate_w, up_w, down_w, perm, fin_rx,
+    x_ref, ids_ref, rw_ref, gain_ref,
+    gate_st, up_st, down_st, gate_tx, up_tx, down_tx,
     tok_tx, rows, hidden, own, part_tx, part_rx, sum_tx, sum_rx, fin_tx,
     ld_sem, w_send, w_recv, tok_send, tok_recv, ex_send, ex_recv, red_send, red_recv,
-    y_send, y_recv, fin_send, fin_recv, out_sem,
+    y_send, y_recv, fin_send, fin_recv, in_sem,
 ):
     f32, bf16 = jnp.float32, jnp.bfloat16
     fs, tp = lax.axis_index("fs"), lax.axis_index("tp")
@@ -94,7 +95,6 @@
     stages = (gate_st, up_st, down_st)
     txs = (gate_tx, up_tx, down_tx)
     lands = (gate_w, up_w, down_w)
-    outs = (gate_out, up_out, down_out)
 
     barrier = pltpu.get_barrier_semaphore()
 
@@ -126,11 +126,18 @@
         at = pl.ds(tgt * n_tp, n_tp)
         return pltpu.make_async_copy(srcs[m].at[at], stages[m].at[at], ld_sem.at[m, tgt])
 
+    small = [
+        pltpu.make_async_copy(src, dst, in_sem.at[i])
+        for i, (src, dst) in enumerate(
+            ((gain_in, gain_ref), (x_in, x_ref), (ids_in, ids_ref), (rw_in, rw_ref))
+        )
+    ]
+    small[0].start()
     for ms, (tgt, _) in plan:
         for m in ms:
             load(m, tgt).start()
-
-    pl.semaphore_wait(barrier, n_dev - 1)
+    for copy in small[1:]:
+        copy.start()
 
     lane = lax.broadcasted_iota(jnp.int32, (toks, extra_lanes), 1).astype(f32)
     lane_pick = jnp.where(lane < group_size, lane, lane - group_size)
@@ -161,6 +168,7 @@
         pltpu.make_async_copy(land, land, sem).wait()
 
 
+    small[0].wait()
     gain = jnp.broadcast_to(as_columns(gain_ref[...])[:, 0:1], gate_in.shape[1:])
 
     def cast(ms, tgt):
@@ -201,8 +209,12 @@
                             txs[m].at[fs * n_tp + tp], block_at(m), w_recv.at[m]
                         ).start()
 
-    step_plan(0, 3)
-
+    step_plan(0, 1)
+    pl.semaphore_wait(barrier, n_dev - 1)
+    step_plan(1, 3)
+
+    for copy in small[1:]:
+        copy.wait()
     x = x_ref[...].astype(f32)
     scale = lax.rsqrt(jnp.mean(x * x, axis=-1, keepdims=True) + norm_eps)
     normed = (x * scale).astype(bf16)
@@ -258,7 +270,6 @@
 
     for m in (0, 1):
         all_here(lands[m], w_recv.at[m])
-        pltpu.make_async_copy(lands[m], outs[m], out_sem.at[m]).start()
 
     @pl.loop(0, n_tp)
     def _(q):
@@ -268,7 +279,6 @@
         hidden[q] = (g / (1.0 + jnp.exp(-g)) * u).astype(bf16)
 
     all_here(down_w, w_recv.at[2])
-    pltpu.make_async_copy(down_w, down_out, out_sem.at[2]).start()
 
     tpf = tp.astype(f32)
 
@@ -335,37 +345,24 @@
         give_back(p)
     for m in range(3):
         all_sent(txs[m], w_send.at[m], n_dev - 1)
-        pltpu.make_async_copy(lands[m], outs[m], out_sem.at[m]).wait()
     all_sent(tok_tx, tok_send, toks - per)
     all_sent(fin_tx, fin_send, toks - per)
     all_here(fin_rx, fin_recv)
 
 
-def write_kernel(perm, fin_rx, gate, up, down, mixed_ref, gate_out, up_out, down_out, gate_v, up_v, down_v, sem_in, sem_out):
-    chunks = sem_in.shape[1]
-    moves = ((gate, gate_v, gate_out), (up, up_v, up_out), (down, down_v, down_out))
-
-    def cut(ref, i):
-        size = ref.shape[0] // chunks
-        return ref.at[pl.ds(i * size, size)]
-
-    def take(m, i):
-        return pltpu.make_async_copy(cut(moves[m][0], i), cut(moves[m][1], i), sem_in.at[m, i])
-
-    def put(m, i):
-        return pltpu.make_async_copy(cut(moves[m][1], i), cut(moves[m][2], i), sem_out.at[m, i])
-
-    every = [(m, i) for m in range(3) for i in range(chunks)]
-    for m, i in every:
-        take(m, i).start()
+def write_kernel(perm, fin_rx, gate, up, down, mixed_ref, gate_out, up_out, down_out, sem):
+    moves = ((gate, gate_out), (up, up_out), (down, down_out))
+
+    def put(m):
+        return pltpu.make_async_copy(moves[m][0], moves[m][1], sem.at[m])
+
+    for m in range(3):
+        put(m).start()
     mixed_ref[...] = jnp.dot(
         perm[...], fin_rx[...], preferred_element_type=jnp.float32
     ).astype(jnp.bfloat16)
-    for m, i in every:
-        take(m, i).wait()
-        put(m, i).start()
-    for m, i in every:
-        put(m, i).wait()
+    for m in range(3):
+        put(m).wait()
 
 
 def shards_fused(n_fs, n_tp, tokens, norm_gain, gate_proj, up_proj, down_proj, expert_ids, route_weight):
@@ -377,29 +374,30 @@
     inner = gc * n_tp
     wide = width + extra_lanes
     vmem = pl.BlockSpec(memory_space=pltpu.VMEM)
-    anywhere = pl.BlockSpec(memory_space=pl.ANY)
+    hbm = pl.BlockSpec(memory_space=pltpu.HBM)
     dma = pltpu.SemaphoreType.DMA
     new_gate, new_up, new_down, perm, returned = pl.pallas_call(
         functools.partial(fused_kernel, n_fs, n_tp),
         out_shape=(
-            jax.ShapeDtypeStruct((width, inner), bf16),
-            jax.ShapeDtypeStruct((width, inner), bf16),
-            jax.ShapeDtypeStruct((inner, width), bf16),
-            jax.ShapeDtypeStruct((toks, toks), bf16),
-            jax.ShapeDtypeStruct((toks, width), bf16),
+            pltpu.VMEM((width, inner), bf16),
+            pltpu.VMEM((width, inner), bf16),
+            pltpu.VMEM((inner, width), bf16),
+            pltpu.VMEM((toks, toks), bf16),
+            pltpu.VMEM((toks, width), bf16),
         ),
-        in_specs=[vmem] * 4 + [anywhere] * 3,
-        out_specs=(anywhere, anywhere, anywhere, vmem, vmem),
+        in_specs=[hbm] * 7,
+        out_specs=(vmem,) * 5,
         scratch_shapes=[
+            pltpu.VMEM(tokens.shape, bf16),
+            pltpu.VMEM((2, toks), jnp.int32),
+            pltpu.VMEM((2, toks), f32),
+            pltpu.VMEM((1, gr), f32),
             pltpu.VMEM((n_dev, gr, gc), f32),
             pltpu.VMEM((n_dev, gr, gc), f32),
             pltpu.VMEM((n_dev, dr, dc), f32),
             pltpu.VMEM((n_dev, gr, gc), bf16),
             pltpu.VMEM((n_dev, gr, gc), bf16),
             pltpu.VMEM((n_dev, dr, dc), bf16),
-            pltpu.VMEM((width, inner), bf16),
-            pltpu.VMEM((width, inner), bf16),
-            pltpu.VMEM((inner, width), bf16),
             pltpu.VMEM((toks, wide), bf16),
             pltpu.VMEM((n_tp, toks, wide), bf16),
             pltpu.VMEM((n_tp, toks, inner), bf16),
@@ -410,12 +408,17 @@
             pltpu.VMEM((toks, width), bf16),
             pltpu.VMEM((toks, width), bf16),
             dma((3, n_fs)), dma((3,)), dma((3,)), dma, dma, dma((3,)), dma((3,)),
-            dma((2,)), dma((2,)), dma((4,)), dma((4,)), dma, dma, dma((3,)),
+            dma((2,)), dma((2,)), dma((4,)), dma((4,)), dma, dma, dma((4,)),
         ],
         compiler_params=pltpu.CompilerParams(
-            collective_id=0, has_side_effects=True, vmem_limit_bytes=60 * 1024 * 1024
+            collective_id=0, has_side_effects=True, vmem_limit_bytes=40 * 1024 * 1024
         ),
-    )(tokens, expert_ids.T, route_weight.T, norm_gain[None, :], gate_proj, up_proj, down_proj)
+    )(*(
+        pltpu.with_memory_space_constraint(a, pltpu.HBM)
+        for a in (
+            tokens, expert_ids.T, route_weight.T, norm_gain[None, :], gate_proj, up_proj, down_proj
+        )
+    ))
     mixed, new_gate, new_up, new_down = pl.pallas_call(
         write_kernel,
         out_shape=(
@@ -424,14 +427,10 @@
             jax.ShapeDtypeStruct((width, inner), bf16),
             jax.ShapeDtypeStruct((inner, width), bf16),
         ),
-        in_specs=[vmem] * 2 + [anywhere] * 3,
-        out_specs=(vmem, anywhere, anywhere, anywhere),
-        scratch_shapes=[
-            pltpu.VMEM((width, inner), bf16),
-            pltpu.VMEM((width, inner), bf16),
-            pltpu.VMEM((inner, width), bf16),
-            dma((3, 4)), dma((3, 4)),
-        ],
+        in_specs=[vmem] * 5,
+        out_specs=(vmem, hbm, hbm, hbm),
+        scratch_shapes=[dma((3,))],
+        compiler_params=pltpu.CompilerParams(vmem_limit_bytes=16 * 1024 * 1024),
     )(perm, returned, new_gate, new_up, new_down)
     return mixed, new_gate[None], new_up[None], new_down[None]
 

time: 189 us -> 185 us (0.979)
  Pallas kernels: 188 us -> 183 us
    pallas_call x1, Pallas kernels: 7.32 us -> 3.54 us  [shards_fused(): pl.pallas_call(write_kernel, out_shape=(jax.ShapeDtypeStruct((toks, width...]
where the time goes in v1:
time: 185 us; the launch traced here: 184 us
  Pallas kernels  183 us (99%)
    pallas_call x1, Pallas kernels, shards_fused(): pl.pallas_call(functools.partial(fused_kernel, n_fs, n_tp), out_shape=(pl...  179 us

profile of v1, /device:TPU:0, one launch (start us, length us, event | category | flops | bytes accessed | tf_op | source)
XLA Modules:
  0.0 183.6 jit_solution(5254710079538082649)
XLA Ops:
  0.6 179.4 %shard_map.102 = (bf16[2048,512]{1,0:T(8,128)(2,1)S(1)}, bf16[2048,512]{1,0:T(8,128)(2,1)S(1)}, bf16[512,2048]{1,0:T(8,128)(2,1)S(1)}, bf16[128,128]{1,0:T(8,128)(2,1)S(1)}, bf16[128,2048]{1,0:T(8,128)(2,1)S(1)}) custom-call(bf16[128,2048]{1,0:T(8,128)(2,1)} %x_in.1, s32[2,128]{1,0:T(2,128)} %bitcast.6, f32[2,128]{1,0:T(2,128)} %bitcast.7, ...), custom_call_target="tpu_custom_call" | custom-call | tf_op jit(solution)/shard_map/pallas_call | solution.py:379
  180.1 3.5 %shard_map.103 = (bf16[128,2048]{1,0:T(8,128)(2,1)}, bf16[2048,512]{1,0:T(8,128)(2,1)}, bf16[2048,512]{1,0:T(8,128)(2,1)}, bf16[512,2048]{1,0:T(8,128)(2,1)}) custom-call(bf16[128,128]{1,0:T(8,128)(2,1)S(1)} %get-tuple-element.13.perm, bf16[128,2048]{1,0:T(8,128)(2,1)S(1)} %get-tuple-element.14.fin_rx, bf16[2048,512]{1,0:T(8,128)(2,1)S(1)} %get-tuple-element.15.gate, ...), custom_call_target="tpu_custom_call" | custom-call | tf_op jit(solution)/shard_map/pallas_call | solution.py:422

commit v2 on v1

--- a/solution.py
+++ b/solution.py
@@ -9,7 +9,7 @@
 
 norm_eps = 1e-06
 group_size = 4
-extra_lanes = 128
+lanes = 128
 MESH = pl.DeviceIdType.MESH
 
 
@@ -78,9 +78,10 @@
     gate_w, up_w, down_w, perm, fin_rx,
     x_ref, ids_ref, rw_ref, gain_ref,
     gate_st, up_st, down_st, gate_tx, up_tx, down_tx,
-    tok_tx, rows, hidden, own, part_tx, part_rx, sum_tx, sum_rx, fin_tx,
-    ld_sem, w_send, w_recv, tok_send, tok_recv, ex_send, ex_recv, red_send, red_recv,
-    y_send, y_recv, fin_send, fin_recv, in_sem,
+    tok_tx, rows, wt_tx, wt_rx, wcol, hidden, own,
+    part_tx, part_rx, sum_tx, sum_rx, fin_tx,
+    in_sem, ld_sem, w_send, w_recv, tok_send, tok_recv, wt_send, wt_recv, ex_send, ex_recv,
+    red_send, red_recv, y_send, y_recv, fin_send, fin_recv,
 ):
     f32, bf16 = jnp.float32, jnp.bfloat16
     fs, tp = lax.axis_index("fs"), lax.axis_index("tp")
@@ -91,6 +92,8 @@
     n_dev = n_fs * n_tp
     toks, width = x_ref.shape
     per = toks // n_fs
+    d_rows, d_cols = down_in.shape[1:]
+    chunks = d_cols // lanes
     srcs = (gate_in, up_in, down_in)
     stages = (gate_st, up_st, down_st)
     txs = (gate_tx, up_tx, down_tx)
@@ -117,10 +120,9 @@
             for at in layers
         ]
 
-    orders = ((outer_far, inner_far), (mate, layer))
-    plan = [
-        (ms, goal) for at in orders for ms in ((0, 1), (2,)) for goal in targets(at)
-    ]
+    far, close = targets((outer_far, inner_far)), targets((mate, layer))
+    ahead = 1
+    plan = far[:ahead] + close + far[ahead:]
 
     def load(m, tgt):
         at = pl.ds(tgt * n_tp, n_tp)
@@ -133,14 +135,14 @@
         )
     ]
     small[0].start()
-    for ms, (tgt, _) in plan:
-        for m in ms:
-            load(m, tgt).start()
-    for copy in small[1:]:
-        copy.start()
-
-    lane = lax.broadcasted_iota(jnp.int32, (toks, extra_lanes), 1).astype(f32)
-    lane_pick = jnp.where(lane < group_size, lane, lane - group_size)
+    for m in (0, 1):
+        load(m, plan[0][0]).start()
+
+    lane_id = lax.broadcasted_iota(jnp.int32, (toks, lanes), 1)
+    row_id = lax.broadcasted_iota(jnp.int32, (toks, lanes), 0)
+    in_group = lax.rem(row_id, per)
+    span_lanes = group_size * per
+
     def as_columns(flat):
         spread_rows = jnp.concatenate([flat] * (8 // flat.shape[0]), axis=0)
         return jnp.transpose(spread_rows)
@@ -148,25 +150,11 @@
     def span(i):
         return pl.ds(pl.multiple_of(i * per, per), per)
 
-    def spread(tx, land, send_sem, recv_sem):
-        @pl.loop(1, n_fs)
-        def _(j):
-            tgt = lax.rem(fs + j, n_fs)
-            pltpu.make_async_remote_copy(
-                src_ref=tx.at[span(tgt)], dst_ref=land.at[span(fs)],
-                send_sem=send_sem, recv_sem=recv_sem,
-                device_id=(tgt, tp), device_id_type=MESH,
-            ).start()
-
-        pltpu.make_async_copy(tx.at[span(fs)], land.at[span(fs)], recv_sem).start()
-
-    def all_sent(tx, sem, count):
-        part = tx.at[pl.ds(0, count)]
+    def all_sent(part, sem):
         pltpu.make_async_copy(part, part, sem).wait()
 
     def all_here(land, sem):
         pltpu.make_async_copy(land, land, sem).wait()
-
 
     small[0].wait()
     gain = jnp.broadcast_to(as_columns(gain_ref[...])[:, 0:1], gate_in.shape[1:])
@@ -186,32 +174,59 @@
         r, c = srcs[m].shape[1:]
         return lands[m].at[pl.ds(pl.multiple_of(fs * r, r), r), pl.ds(pl.multiple_of(tp * c, c), c)]
 
-    def send(ms, tgt, first):
-        for t in range(first, n_tp):
+    def send(tgt, same):
+        for t in range(1 if same else 0, n_tp):
             to = lax.rem(tp + t, n_tp)
-            for m in ms:
+            for m in (0, 1):
                 pltpu.make_async_remote_copy(
                     src_ref=txs[m].at[tgt * n_tp + to], dst_ref=block_at(m),
                     send_sem=w_send.at[m], recv_sem=w_recv.at[m],
                     device_id=(tgt, to), device_id_type=MESH,
                 ).start()
+        if same:
+            for m in (0, 1):
+                pltpu.make_async_copy(
+                    txs[m].at[fs * n_tp + tp], block_at(m), w_recv.at[m]
+                ).start()
 
     def step_plan(first, last):
         for k in range(first, last):
             if k < len(plan):
-                cast(plan[k][0], plan[k][1][0])
+                cast((0, 1), plan[k][0])
             if k > 0:
-                ms, (tgt, same) = plan[k - 1]
-                send(ms, tgt, 1 if same else 0)
-                if same:
-                    for m in ms:
-                        pltpu.make_async_copy(
-                            txs[m].at[fs * n_tp + tp], block_at(m), w_recv.at[m]
-                        ).start()
+                send(*plan[k - 1])
+
+    def chunk_block(k):
+        return down_w.at[
+            pl.ds(pl.multiple_of(fs * d_rows, d_rows), d_rows),
+            pl.ds(pl.multiple_of(tp * d_cols + k * lanes, lanes), lanes),
+        ]
+
+    def send_chunk(k):
+        for tgt, same in close + far:
+            for t in range(1 if same else 0, n_tp):
+                to = lax.rem(tp + t, n_tp)
+                pltpu.make_async_remote_copy(
+                    src_ref=down_tx.at[tgt * n_tp + to, :, pl.ds(k * lanes, lanes)],
+                    dst_ref=chunk_block(k),
+                    send_sem=w_send.at[2 + k], recv_sem=w_recv.at[2 + k],
+                    device_id=(tgt, to), device_id_type=MESH,
+                ).start()
+            if same:
+                pltpu.make_async_copy(
+                    down_tx.at[fs * n_tp + tp, :, pl.ds(k * lanes, lanes)],
+                    chunk_block(k), w_recv.at[2 + k],
+                ).start()
 
     step_plan(0, 1)
+    for copy in small[1:]:
+        copy.start()
+    for ms in ((0, 1), (2,)):
+        for tgt, _ in plan[1:] if ms[0] == 0 else plan:
+            for m in ms:
+                load(m, tgt).start()
     pl.semaphore_wait(barrier, n_dev - 1)
-    step_plan(1, 3)
+    step_plan(1, ahead + 1)
 
     for copy in small[1:]:
         copy.wait()
@@ -228,28 +243,51 @@
     rank = jnp.dot(before.astype(bf16), named.astype(bf16), preferred_element_type=f32)
     place = jnp.where(rank == slot - slot_grp * per, named, 0.0).astype(bf16)
     perm[...] = place
+    by_slot = (((0,), (0,)), ((), ()))
+    tok_tx[...] = lax.dot_general(
+        place, normed, by_slot, preferred_element_type=f32
+    ).astype(bf16)
+
+    @pl.loop(1, n_fs)
+    def _(j):
+        tgt = lax.rem(fs + j, n_fs)
+        pltpu.make_async_remote_copy(
+            src_ref=tok_tx.at[span(tgt)], dst_ref=rows.at[tp, span(fs)],
+            send_sem=tok_send, recv_sem=tok_recv,
+            device_id=(tgt, tp), device_id_type=MESH,
+        ).start()
+
+    pltpu.make_async_copy(tok_tx.at[span(fs)], rows.at[tp, span(fs)], tok_recv).start()
+
+    lane_pick = (lax.rem(lane_id, span_lanes) // per).astype(f32)
     local = idf - grp * group_size
     rw = as_columns(rw_ref[...])
     wv = jnp.where(local[:, 0:1] == lane_pick, rw[:, 0:1], 0.0) + jnp.where(
         local[:, 1:2] == lane_pick, rw[:, 1:2], 0.0
     )
-    high = wv.astype(bf16)
-    low = (wv - high.astype(f32)).astype(bf16)
-    aug = jnp.where(
-        lane < group_size,
-        high.astype(f32),
-        jnp.where(lane < 2 * group_size, low.astype(f32), 0.0),
-    ).astype(bf16)
-    by_slot = (((0,), (0,)), ((), ()))
-    tok_tx[:, 0:width] = lax.dot_general(
-        place, normed, by_slot, preferred_element_type=f32
-    ).astype(bf16)
-    tok_tx[:, width:] = lax.dot_general(
-        place, aug, by_slot, preferred_element_type=f32
-    ).astype(bf16)
-    spread(tok_tx, rows.at[tp], tok_send, tok_recv)
-
-    step_plan(3, len(plan) + 1)
+    high = wv.astype(bf16).astype(f32)
+    aug = jnp.where(lane_id < span_lanes, high, wv - high).astype(bf16)
+    by_row = lax.dot_general(place, aug, by_slot, preferred_element_type=f32)
+    by_row = jnp.where(lax.rem(lane_id, per) == in_group, by_row, 0.0)
+    wt_tx[...] = jnp.sum(by_row.reshape(n_fs, per, lanes), axis=1, keepdims=True)
+
+    @pl.loop(1, n_dev)
+    def _(k):
+        dev = lax.rem(fs * n_tp + tp + k, n_dev)
+        tgt = dev // n_tp
+        pltpu.make_async_remote_copy(
+            src_ref=wt_tx.at[tgt], dst_ref=wt_rx.at[tp, fs],
+            send_sem=wt_send, recv_sem=wt_recv,
+            device_id=(tgt, lax.rem(dev, n_tp)), device_id_type=MESH,
+        ).start()
+
+    pltpu.make_async_copy(wt_tx.at[fs], wt_rx.at[tp, fs], wt_recv).start()
+
+    step_plan(ahead + 1, len(plan) + 1)
+    for tgt, _ in plan:
+        cast((2,), tgt)
+    for k in range(chunks - 1):
+        send_chunk(k)
 
     def swap(src, dst, to, send_sem, recv_sem):
         return pltpu.make_async_remote_copy(
@@ -263,41 +301,28 @@
     near = swap(rows.at[tp], rows.at[tp], partner, ex_send.at[1], ex_recv.at[1])
     near.start()
     cross.wait()
-    far = swap(rows.at[across], rows.at[across], partner, ex_send.at[2], ex_recv.at[2])
-    far.start()
+    other = swap(rows.at[across], rows.at[across], partner, ex_send.at[2], ex_recv.at[2])
+    other.start()
     near.wait()
-    far.wait()
+    other.wait()
+    all_here(wt_rx, wt_recv)
+    mine = lax.rem(lane_id, span_lanes) == tp * per + in_group
+
+    @pl.loop(0, n_tp)
+    def _(q):
+        w = jnp.broadcast_to(wt_rx[q], (n_fs, per, lanes)).reshape(toks, lanes)
+        wcol[q] = jnp.broadcast_to(
+            jnp.sum(jnp.where(mine, w, 0.0), axis=-1, keepdims=True), (toks, lanes)
+        )
 
     for m in (0, 1):
         all_here(lands[m], w_recv.at[m])
 
     @pl.loop(0, n_tp)
     def _(q):
-        block = rows[q, :, 0:width]
-        g = jnp.dot(block, gate_w[...], preferred_element_type=f32)
-        u = jnp.dot(block, up_w[...], preferred_element_type=f32)
+        g = jnp.dot(rows[q], gate_w[...], preferred_element_type=f32)
+        u = jnp.dot(rows[q], up_w[...], preferred_element_type=f32)
         hidden[q] = (g / (1.0 + jnp.exp(-g)) * u).astype(bf16)
-
-    all_here(down_w, w_recv.at[2])
-
-    tpf = tp.astype(f32)
-
-    def partial(q):
-        w = jnp.sum(
-            jnp.where(lane_pick == tpf, rows[q, :, width:].astype(f32), 0.0),
-            axis=-1, keepdims=True,
-        )
-        return jnp.dot(hidden[q], down_w[...], preferred_element_type=f32) * w
-
-    def reduce_near(i, p):
-        return swap(part_tx.at[i], part_rx.at[i], partner, red_send.at[i], red_recv.at[i])
-
-    def give(i, side):
-        part_tx[i] = partial(side * 2 + 1 - core).astype(bf16)
-        reduce_near(i, partner).start()
-        own[i] = partial(side * 2 + core)
-        reduce_near(i, partner).wait()
-        own[i] = own[i] + part_rx[i].astype(f32)
 
     pieces = 4
     step = n_fs // pieces
@@ -308,60 +333,101 @@
     def piece_rows(p):
         return pl.ds(pl.multiple_of(piece(p) * step * per, step * per), step * per)
 
-    def over(p):
+    def reduce_near(k):
+        return swap(part_tx.at[k], part_rx.at[k], partner, red_send.at[k], red_recv.at[k])
+
+    def over(k, p):
         at = piece_rows(p)
-        return swap(sum_tx.at[at], sum_rx.at[at], across, y_send.at[p], y_recv.at[p])
-
-    give(0, 1 - pair)
-    for p in range(pieces):
-        at = piece_rows(p)
-        sum_tx[at] = own[0, at].astype(bf16)
-    for p in range(pieces):
-        over(p).start()
-    give(1, pair)
-
-    def give_back(p):
-        for i in range(step):
-            to = piece(p) * step + i
-
-            @pl.when(to != fs)
-            def _():
-                pltpu.make_async_remote_copy(
-                    src_ref=fin_tx.at[span(to)], dst_ref=fin_rx.at[span(fs)],
-                    send_sem=fin_send, recv_sem=fin_recv,
-                    device_id=(to, tp), device_id_type=MESH,
-                ).start()
-
-            @pl.when(to == fs)
-            def _():
-                pltpu.make_async_copy(
-                    fin_tx.at[span(fs)], fin_rx.at[span(fs)], fin_recv
-                ).start()
-
-    for p in range(pieces):
-        over(p).wait()
-        at = piece_rows(p)
-        fin_tx[at] = (own[1, at] + sum_rx[at].astype(f32)).astype(bf16)
-        give_back(p)
-    for m in range(3):
-        all_sent(txs[m], w_send.at[m], n_dev - 1)
-    all_sent(tok_tx, tok_send, toks - per)
-    all_sent(fin_tx, fin_send, toks - per)
+        return swap(
+            sum_tx.at[k, at], sum_rx.at[k, at], across, y_send.at[k, p], y_recv.at[k, p]
+        )
+
+    def multiply(k):
+        columns = jnp.concatenate(
+            [down_w[:, pl.ds(t * d_cols + k * lanes, lanes)] for t in range(n_tp)], axis=1
+        )
+
+        def partial(q):
+            w = jnp.concatenate([wcol[q]] * n_tp, axis=1)
+            return jnp.dot(hidden[q], columns, preferred_element_type=f32) * w
+
+        for side in range(2):
+            part_tx[k, side] = partial(side * 2 + 1 - core).astype(bf16)
+        reduce_near(k).start()
+        own[k, 0] = partial((1 - pair) * 2 + core)
+        own[k, 1] = partial(pair * 2 + core)
+
+    def cross_over(k):
+        reduce_near(k).wait()
+        for p in range(pieces):
+            at = piece_rows(p)
+            sum_tx[k, at] = (own[k, 0, at] + part_rx[k, 1 - pair, at].astype(f32)).astype(bf16)
+            over(k, p).start()
+
+    def give_back(k):
+        for p in range(pieces):
+            at = piece_rows(p)
+            own_part = own[k, 1, at] + part_rx[k, pair, at].astype(f32)
+            over(k, p).wait()
+            fin_tx[k, at] = (own_part + sum_rx[k, at].astype(f32)).astype(bf16)
+            for i in range(step):
+                to = piece(p) * step + i
+
+                @pl.when(to != fs)
+                def _():
+                    pltpu.make_async_remote_copy(
+                        src_ref=fin_tx.at[k, span(to)], dst_ref=fin_rx.at[k, span(fs)],
+                        send_sem=fin_send, recv_sem=fin_recv,
+                        device_id=(to, tp), device_id_type=MESH,
+                    ).start()
+
+                @pl.when(to == fs)
+                def _():
+                    pltpu.make_async_copy(
+                        fin_tx.at[k, span(fs)], fin_rx.at[k, span(fs)], fin_recv
+                    ).start()
+
+    chunk_area = down_w.at[:, pl.ds(0, n_tp * lanes)]
+    for k in range(chunks):
+        all_here(chunk_area, w_recv.at[2 + k])
+        multiply(k)
+        if k > 0:
+            give_back(k - 1)
+        if k == 1:
+            send_chunk(chunks - 1)
+        cross_over(k)
+    give_back(chunks - 1)
+
+    for m in (0, 1):
+        all_sent(txs[m].at[pl.ds(0, n_dev - 1)], w_send.at[m])
+    for k in range(chunks):
+        all_sent(down_tx.at[pl.ds(0, n_dev - 1), :, pl.ds(0, lanes)], w_send.at[2 + k])
+    all_sent(tok_tx.at[pl.ds(0, toks - per)], tok_send)
+    all_sent(wt_rx.at[0, pl.ds(0, n_fs - 1)], wt_send)
+    for _ in range(n_tp - 1):
+        all_sent(wt_rx.at[0], wt_send)
+    all_sent(fin_tx.at[:, pl.ds(0, toks - per)], fin_send)
     all_here(fin_rx, fin_recv)
 
 
-def write_kernel(perm, fin_rx, gate, up, down, mixed_ref, gate_out, up_out, down_out, sem):
-    moves = ((gate, gate_out), (up, up_out), (down, down_out))
+def write_kernel(perm, fin_rx, gate, up, down, mixed_out, gate_out, up_out, down_out, mixed, sem):
+    chunks, _, wide = fin_rx.shape
+    blocks = wide // lanes
+    moves = ((gate, gate_out), (up, up_out), (down, down_out), (mixed, mixed_out))
 
     def put(m):
         return pltpu.make_async_copy(moves[m][0], moves[m][1], sem.at[m])
 
     for m in range(3):
         put(m).start()
-    mixed_ref[...] = jnp.dot(
-        perm[...], fin_rx[...], preferred_element_type=jnp.float32
-    ).astype(jnp.bfloat16)
-    for m in range(3):
+    for k in range(chunks):
+        part = jnp.dot(
+            perm[...], fin_rx[k], preferred_element_type=jnp.float32
+        ).astype(jnp.bfloat16)
+        for t in range(blocks):
+            mixed[:, pl.ds((t * chunks + k) * lanes, lanes)] = part[:, t * lanes:(t + 1) * lanes]
+    put(3).start()
+    for m in range(4):
         put(m).wait()
 
 
@@ -372,7 +438,7 @@
     _, gr, gc = gate_proj.shape
     _, dr, dc = down_proj.shape
     inner = gc * n_tp
-    wide = width + extra_lanes
+    chunks, wide = dc // lanes, n_tp * lanes
     vmem = pl.BlockSpec(memory_space=pltpu.VMEM)
     hbm = pl.BlockSpec(memory_space=pltpu.HBM)
     dma = pltpu.SemaphoreType.DMA
@@ -383,7 +449,7 @@
             pltpu.VMEM((width, inner), bf16),
             pltpu.VMEM((inner, width), bf16),
             pltpu.VMEM((toks, toks), bf16),
-            pltpu.VMEM((toks, width), bf16),
+            pltpu.VMEM((chunks, toks, wide), bf16),
         ),
         in_specs=[hbm] * 7,
         out_specs=(vmem,) * 5,
@@ -398,20 +464,24 @@
             pltpu.VMEM((n_dev, gr, gc), bf16),
             pltpu.VMEM((n_dev, gr, gc), bf16),
             pltpu.VMEM((n_dev, dr, dc), bf16),
-            pltpu.VMEM((toks, wide), bf16),
-            pltpu.VMEM((n_tp, toks, wide), bf16),
+            pltpu.VMEM((toks, width), bf16),
+            pltpu.VMEM((n_tp, toks, width), bf16),
+            pltpu.VMEM((n_fs, 1, lanes), f32),
+            pltpu.VMEM((n_tp, n_fs, 1, lanes), f32),
+            pltpu.VMEM((n_tp, toks, lanes), f32),
             pltpu.VMEM((n_tp, toks, inner), bf16),
-            pltpu.VMEM((2, toks, width), f32),
-            pltpu.VMEM((2, toks, width), bf16),
-            pltpu.VMEM((2, toks, width), bf16),
-            pltpu.VMEM((toks, width), bf16),
-            pltpu.VMEM((toks, width), bf16),
-            pltpu.VMEM((toks, width), bf16),
-            dma((3, n_fs)), dma((3,)), dma((3,)), dma, dma, dma((3,)), dma((3,)),
-            dma((2,)), dma((2,)), dma((4,)), dma((4,)), dma, dma, dma((4,)),
+            pltpu.VMEM((chunks, 2, toks, wide), f32),
+            pltpu.VMEM((chunks, 2, toks, wide), bf16),
+            pltpu.VMEM((chunks, 2, toks, wide), bf16),
+            pltpu.VMEM((chunks, toks, wide), bf16),
+            pltpu.VMEM((chunks, toks, wide), bf16),
+            pltpu.VMEM((chunks, toks, wide), bf16),
+            dma((4,)), dma((3, n_fs)), dma((2 + chunks,)), dma((2 + chunks,)), dma, dma, dma, dma,
+            dma((3,)), dma((3,)), dma((chunks,)), dma((chunks,)), dma((chunks, 4)),
+            dma((chunks, 4)), dma, dma,
         ],
         compiler_params=pltpu.CompilerParams(
-            collective_id=0, has_side_effects=True, vmem_limit_bytes=40 * 1024 * 1024
+            collective_id=0, has_side_effects=True, vmem_limit_bytes=46 * 1024 * 1024
         ),
     )(*(
         pltpu.with_memory_space_constraint(a, pltpu.HBM)
@@ -428,8 +498,8 @@
             jax.ShapeDtypeStruct((inner, width), bf16),
         ),
         in_specs=[vmem] * 5,
-        out_specs=(vmem, hbm, hbm, hbm),
-        scratch_shapes=[dma((3,))],
+        out_specs=(hbm,) * 4,
+        scratch_shapes=[pltpu.VMEM((toks, width), bf16), dma((4,))],
         compiler_params=pltpu.CompilerParams(vmem_limit_bytes=16 * 1024 * 1024),
     )(perm, returned, new_gate, new_up, new_down)
     return mixed, new_gate[None], new_up[None], new_down[None]
@@ -447,6 +517,7 @@
         and down_proj.shape[2] % 128 == 0
         and gate_proj.shape[1] % 16 == 0
         and down_proj.shape[1] % 16 == 0
+        and 2 * group_size * toks == lanes * n_fs
     )
     if whole_tiles:
         return shards_fused(n_fs, n_tp, *args)

time: 185 us -> 175 us (0.946)
  Pallas kernels: 183 us -> 174 us
    pallas_call x1, Pallas kernels: 179 us -> 171 us  [shards_fused(): pl.pallas_call(functools.partial(fused_kernel, n_fs, n_tp), out_shape=(pl...]
where the time goes in v2:
time: 175 us
  Pallas kernels  174 us (99%)
    pallas_call x1, Pallas kernels, shards_fused(): pl.pallas_call(functools.partial(fused_kernel, n_fs, n_tp), out_shape=(pl...  171 us

profile of v2, /device:TPU:0, one launch (start us, length us, event | category | flops | bytes accessed | tf_op | source)
XLA Modules:
  0.0 174.8 jit_solution(17252559014846646733)
XLA Ops:
  0.6 171.3 %shard_map.102 = (bf16[2048,512]{1,0:T(8,128)(2,1)S(1)}, bf16[2048,512]{1,0:T(8,128)(2,1)S(1)}, bf16[512,2048]{1,0:T(8,128)(2,1)S(1)}, bf16[128,128]{1,0:T(8,128)(2,1)S(1)}, bf16[4,128,512]{2,1,0:T(8,128)(2,1)S(1)}) custom-call(bf16[128,2048]{1,0:T(8,128)(2,1)} %x_in.1, s32[2,128]{1,0:T(2,128)} %bitcast.6, f32[2,128]{1,0:T(2,128)} %bitcast.7, ...), custom_call_target="tpu_custom_call" | custom-call | tf_op jit(solution)/shard_map/pallas_call | solution.py:445
  172.0 2.9 %shard_map.103 = (bf16[128,2048]{1,0:T(8,128)(2,1)}, bf16[2048,512]{1,0:T(8,128)(2,1)}, bf16[2048,512]{1,0:T(8,128)(2,1)}, bf16[512,2048]{1,0:T(8,128)(2,1)}) custom-call(bf16[128,128]{1,0:T(8,128)(2,1)S(1)} %get-tuple-element.13.perm, bf16[4,128,512]{2,1,0:T(8,128)(2,1)S(1)} %get-tuple-element.14.fin_rx, bf16[2048,512]{1,0:T(8,128)(2,1)S(1)} %get-tuple-element.15.gate, ...), custom_call_target="tpu_custom_call" | custom-call | tf_op jit(solution)/shard_map/pallas_call | solution.py:492

commit v3 on v2

--- a/solution.py
+++ b/solution.py
@@ -77,11 +77,11 @@
     x_in, ids_in, rw_in, gain_in, gate_in, up_in, down_in,
     gate_w, up_w, down_w, perm, fin_rx,
     x_ref, ids_ref, rw_ref, gain_ref,
-    gate_st, up_st, down_st, gate_tx, up_tx, down_tx,
+    gate_st, up_st, down_st, gate_tx, up_tx, down_tx, early_st, early_tx,
     tok_tx, rows, wt_tx, wt_rx, wcol, hidden, own,
     part_tx, part_rx, sum_tx, sum_rx, fin_tx,
     in_sem, ld_sem, w_send, w_recv, tok_send, tok_recv, wt_send, wt_recv, ex_send, ex_recv,
-    red_send, red_recv, y_send, y_recv, fin_send, fin_recv,
+    red_send, red_recv, y_send, y_recv, fin_send, fin_recv, early_sem, met_sem,
 ):
     f32, bf16 = jnp.float32, jnp.bfloat16
     fs, tp = lax.axis_index("fs"), lax.axis_index("tp")
@@ -99,23 +99,34 @@
     txs = (gate_tx, up_tx, down_tx)
     lands = (gate_w, up_w, down_w)
 
-    barrier = pltpu.get_barrier_semaphore()
-
-    @pl.loop(1, n_dev)
-    def _(k):
-        dev = lax.rem(fs * n_tp + tp + k, n_dev)
-        pl.semaphore_signal(
-            barrier, inc=1, device_id=(dev // n_tp, lax.rem(dev, n_tp)), device_id_type=MESH
-        )
-
     quarter = n_fs // 4
     layer, col = fs // quarter, lax.rem(fs, quarter)
+    plane = quarter * n_tp
+    barrier = pltpu.get_barrier_semaphore()
+
+    def greet_plane(sem):
+        @pl.loop(1, plane)
+        def _(k):
+            at = lax.rem(col * n_tp + tp + k, plane)
+            pl.semaphore_signal(
+                sem, inc=1,
+                device_id=(layer * quarter + at // n_tp, lax.rem(at, n_tp)),
+                device_id_type=MESH,
+            )
+
+    for k in range(1, 4):
+        pl.semaphore_signal(
+            barrier, inc=1,
+            device_id=(lax.rem(layer + k, 4) * quarter + col, tp), device_id_type=MESH,
+        )
+    greet_plane(barrier)
     half = layer // 2
     inner_far, outer_far, mate = 2 - half, 3 - 3 * half, 4 * half + 1 - layer
 
     def targets(layers):
         return [
-            (at * quarter + lax.rem(col + 1 + i, quarter), at is layer and i == quarter - 1)
+            (at * quarter + lax.rem(col + 1 + i, quarter), at is layer and i == quarter - 1,
+             i == quarter - 1 and at is not layer and at is not mate)
             for i in range(quarter)
             for at in layers
         ]
@@ -134,7 +145,17 @@
             ((gain_in, gain_ref), (x_in, x_ref), (ids_in, ids_ref), (rw_in, rw_ref))
         )
     ]
+    early = [(m, j) for j in range(2) for m in (0, 1)]
+    lines = (inner_far * quarter + col, outer_far * quarter + col)
+
+    def load_early(m, j):
+        return pltpu.make_async_copy(
+            srcs[m].at[lines[j] * n_tp + tp], early_st.at[m, j], early_sem.at[m, j]
+        )
+
     small[0].start()
+    for m, j in early:
+        load_early(m, j).start()
     for m in (0, 1):
         load(m, plan[0][0]).start()
 
@@ -174,8 +195,8 @@
         r, c = srcs[m].shape[1:]
         return lands[m].at[pl.ds(pl.multiple_of(fs * r, r), r), pl.ds(pl.multiple_of(tp * c, c), c)]
 
-    def send(tgt, same):
-        for t in range(1 if same else 0, n_tp):
+    def send(tgt, same, begun):
+        for t in range(1 if same or begun else 0, n_tp):
             to = lax.rem(tp + t, n_tp)
             for m in (0, 1):
                 pltpu.make_async_remote_copy(
@@ -203,7 +224,7 @@
         ]
 
     def send_chunk(k):
-        for tgt, same in close + far:
+        for tgt, same, _ in close + far:
             for t in range(1 if same else 0, n_tp):
                 to = lax.rem(tp + t, n_tp)
                 pltpu.make_async_remote_copy(
@@ -218,14 +239,25 @@
                     chunk_block(k), w_recv.at[2 + k],
                 ).start()
 
+    for m, j in early:
+        load_early(m, j).wait()
+        early_tx[m, j] = (early_st[m, j] * gain).astype(bf16)
+    pl.semaphore_wait(barrier, plane + 2)
+    greet_plane(met_sem)
+    for m, j in early:
+        pltpu.make_async_remote_copy(
+            src_ref=early_tx.at[m, j], dst_ref=block_at(m),
+            send_sem=w_send.at[m], recv_sem=w_recv.at[m],
+            device_id=(lines[j], tp), device_id_type=MESH,
+        ).start()
     step_plan(0, 1)
     for copy in small[1:]:
         copy.start()
     for ms in ((0, 1), (2,)):
-        for tgt, _ in plan[1:] if ms[0] == 0 else plan:
+        for tgt, _, _ in plan[1:] if ms[0] == 0 else plan:
             for m in ms:
                 load(m, tgt).start()
-    pl.semaphore_wait(barrier, n_dev - 1)
+    pl.semaphore_wait(met_sem, plane - 1)
     step_plan(1, ahead + 1)
 
     for copy in small[1:]:
@@ -284,9 +316,9 @@
     pltpu.make_async_copy(wt_tx.at[fs], wt_rx.at[tp, fs], wt_recv).start()
 
     step_plan(ahead + 1, len(plan) + 1)
-    for tgt, _ in plan:
+    for tgt, _, _ in plan:
         cast((2,), tgt)
-    for k in range(chunks - 1):
+    for k in range(chunks):
         send_chunk(k)
 
     def swap(src, dst, to, send_sem, recv_sem):
@@ -391,11 +423,10 @@
     for k in range(chunks):
         all_here(chunk_area, w_recv.at[2 + k])
         multiply(k)
-        if k > 0:
-            give_back(k - 1)
-        if k == 1:
-            send_chunk(chunks - 1)
+        if k > 1:
+            give_back(k - 2)
         cross_over(k)
+    give_back(chunks - 2)
     give_back(chunks - 1)
 
     for m in (0, 1):
@@ -464,6 +495,8 @@
             pltpu.VMEM((n_dev, gr, gc), bf16),
             pltpu.VMEM((n_dev, gr, gc), bf16),
             pltpu.VMEM((n_dev, dr, dc), bf16),
+            pltpu.VMEM((2, 2, gr, gc), f32),
+            pltpu.VMEM((2, 2, gr, gc), bf16),
             pltpu.VMEM((toks, width), bf16),
             pltpu.VMEM((n_tp, toks, width), bf16),
             pltpu.VMEM((n_fs, 1, lanes), f32),
@@ -478,10 +511,10 @@
             pltpu.VMEM((chunks, toks, wide), bf16),
             dma((4,)), dma((3, n_fs)), dma((2 + chunks,)), dma((2 + chunks,)), dma, dma, dma, dma,
             dma((3,)), dma((3,)), dma((chunks,)), dma((chunks,)), dma((chunks, 4)),
-            dma((chunks, 4)), dma, dma,
+            dma((chunks, 4)), dma, dma, dma((2, 2)), pltpu.SemaphoreType.REGULAR,
         ],
         compiler_params=pltpu.CompilerParams(
-            collective_id=0, has_side_effects=True, vmem_limit_bytes=46 * 1024 * 1024
+            collective_id=0, has_side_effects=True, vmem_limit_bytes=47 * 1024 * 1024
         ),
     )(*(
         pltpu.with_memory_space_constraint(a, pltpu.HBM)

time: 175 us -> 171 us (0.977)
  Pallas kernels: 174 us -> 170 us
    pallas_call x1, Pallas kernels: 171 us -> 167 us  [shards_fused(): pl.pallas_call(functools.partial(fused_kernel, n_fs, n_tp), out_shape=(pl...]
where the time goes in v3:
time: 171 us
  Pallas kernels  170 us (99%)
    pallas_call x1, Pallas kernels, shards_fused(): pl.pallas_call(functools.partial(fused_kernel, n_fs, n_tp), out_shape=(pl...  167 us

profile of v3, /device:TPU:0, one launch (start us, length us, event | category | flops | bytes accessed | tf_op | source)
XLA Modules:
  0.0 170.8 jit_solution(2950079881207602465)
XLA Ops:
  0.6 167.3 %shard_map.102 = (bf16[2048,512]{1,0:T(8,128)(2,1)S(1)}, bf16[2048,512]{1,0:T(8,128)(2,1)S(1)}, bf16[512,2048]{1,0:T(8,128)(2,1)S(1)}, bf16[128,128]{1,0:T(8,128)(2,1)S(1)}, bf16[4,128,512]{2,1,0:T(8,128)(2,1)S(1)}) custom-call(bf16[128,2048]{1,0:T(8,128)(2,1)} %x_in.1, s32[2,128]{1,0:T(2,128)} %bitcast.6, f32[2,128]{1,0:T(2,128)} %bitcast.7, ...), custom_call_target="tpu_custom_call" | custom-call | tf_op jit(solution)/shard_map/pallas_call | solution.py:476
  168.0 2.9 %shard_map.103 = (bf16[128,2048]{1,0:T(8,128)(2,1)}, bf16[2048,512]{1,0:T(8,128)(2,1)}, bf16[2048,512]{1,0:T(8,128)(2,1)}, bf16[512,2048]{1,0:T(8,128)(2,1)}) custom-call(bf16[128,128]{1,0:T(8,128)(2,1)S(1)} %get-tuple-element.13.perm, bf16[4,128,512]{2,1,0:T(8,128)(2,1)S(1)} %get-tuple-element.14.fin_rx, bf16[2048,512]{1,0:T(8,128)(2,1)S(1)} %get-tuple-element.15.gate, ...), custom_call_target="tpu_custom_call" | custom-call | tf_op jit(solution)/shard_map/pallas_call | solution.py:525

commit v4 on v3

--- a/solution.py
+++ b/solution.py
@@ -10,6 +10,7 @@
 norm_eps = 1e-06
 group_size = 4
 lanes = 128
+last_cuts = 2
 MESH = pl.DeviceIdType.MESH
 
 
@@ -217,26 +218,27 @@
             if k > 0:
                 send(*plan[k - 1])
 
-    def chunk_block(k):
-        return down_w.at[
-            pl.ds(pl.multiple_of(fs * d_rows, d_rows), d_rows),
+    cuts = [(k, 0, d_rows) for k in range(chunks - 1)]
+    cuts += [(chunks - 1, i * d_rows // last_cuts, d_rows // last_cuts) for i in range(last_cuts)]
+
+    def send_cut(c):
+        k, row, count = cuts[c]
+        piece_of = (pl.ds(row, count), pl.ds(k * lanes, lanes))
+        land = down_w.at[
+            pl.ds(pl.multiple_of(fs * d_rows + row, count), count),
             pl.ds(pl.multiple_of(tp * d_cols + k * lanes, lanes), lanes),
         ]
-
-    def send_chunk(k):
         for tgt, same, _ in close + far:
             for t in range(1 if same else 0, n_tp):
                 to = lax.rem(tp + t, n_tp)
                 pltpu.make_async_remote_copy(
-                    src_ref=down_tx.at[tgt * n_tp + to, :, pl.ds(k * lanes, lanes)],
-                    dst_ref=chunk_block(k),
-                    send_sem=w_send.at[2 + k], recv_sem=w_recv.at[2 + k],
+                    src_ref=down_tx.at[(tgt * n_tp + to,) + piece_of], dst_ref=land,
+                    send_sem=w_send.at[2 + c], recv_sem=w_recv.at[2 + c],
                     device_id=(tgt, to), device_id_type=MESH,
                 ).start()
             if same:
                 pltpu.make_async_copy(
-                    down_tx.at[fs * n_tp + tp, :, pl.ds(k * lanes, lanes)],
-                    chunk_block(k), w_recv.at[2 + k],
+                    down_tx.at[(fs * n_tp + tp,) + piece_of], land, w_recv.at[2 + c]
                 ).start()
 
     for m, j in early:
@@ -318,8 +320,8 @@
     step_plan(ahead + 1, len(plan) + 1)
     for tgt, _, _ in plan:
         cast((2,), tgt)
-    for k in range(chunks):
-        send_chunk(k)
+    for c in range(len(cuts)):
+        send_cut(c)
 
     def swap(src, dst, to, send_sem, recv_sem):
         return pltpu.make_async_remote_copy(
@@ -396,8 +398,8 @@
             sum_tx[k, at] = (own[k, 0, at] + part_rx[k, 1 - pair, at].astype(f32)).astype(bf16)
             over(k, p).start()
 
-    def give_back(k):
-        for p in range(pieces):
+    def give_back(k, ps=tuple(range(4))):
+        for p in ps:
             at = piece_rows(p)
             own_part = own[k, 1, at] + part_rx[k, pair, at].astype(f32)
             over(k, p).wait()
@@ -419,20 +421,32 @@
                         fin_tx.at[k, span(fs)], fin_rx.at[k, span(fs)], fin_recv
                     ).start()
 
-    chunk_area = down_w.at[:, pl.ds(0, n_tp * lanes)]
-    for k in range(chunks):
-        all_here(chunk_area, w_recv.at[2 + k])
+    def cut_here(c):
+        area = down_w.at[pl.ds(0, n_fs * cuts[c][2]), pl.ds(0, n_tp * lanes)]
+        all_here(area, w_recv.at[2 + c])
+
+    for k in range(chunks - 1):
+        cut_here(k)
         multiply(k)
-        if k > 1:
-            give_back(k - 2)
         cross_over(k)
-    give_back(chunks - 2)
-    give_back(chunks - 1)
+    last = chunks - 1
+    cut_here(last)
+    give_back(0)
+    give_back(1, (0,))
+    cut_here(last + 1)
+    multiply(last)
+    cross_over(last)
+    give_back(last - 1, (0,))
+    give_back(last, (0,))
+    for k in range(1, chunks):
+        give_back(k, (1, 2, 3))
 
     for m in (0, 1):
         all_sent(txs[m].at[pl.ds(0, n_dev - 1)], w_send.at[m])
-    for k in range(chunks):
-        all_sent(down_tx.at[pl.ds(0, n_dev - 1), :, pl.ds(0, lanes)], w_send.at[2 + k])
+    for c, (_, _, count) in enumerate(cuts):
+        all_sent(
+            down_tx.at[pl.ds(0, n_dev - 1), pl.ds(0, count), pl.ds(0, lanes)], w_send.at[2 + c]
+        )
     all_sent(tok_tx.at[pl.ds(0, toks - per)], tok_send)
     all_sent(wt_rx.at[0, pl.ds(0, n_fs - 1)], wt_send)
     for _ in range(n_tp - 1):
@@ -509,7 +523,7 @@
             pltpu.VMEM((chunks, toks, wide), bf16),
             pltpu.VMEM((chunks, toks, wide), bf16),
             pltpu.VMEM((chunks, toks, wide), bf16),
-            dma((4,)), dma((3, n_fs)), dma((2 + chunks,)), dma((2 + chunks,)), dma, dma, dma, dma,
+            dma((4,)), dma((3, n_fs)), dma((1 + chunks + last_cuts,)), dma((1 + chunks + last_cuts,)), dma, dma, dma, dma,
             dma((3,)), dma((3,)), dma((chunks,)), dma((chunks,)), dma((chunks, 4)),
             dma((chunks, 4)), dma, dma, dma((2, 2)), pltpu.SemaphoreType.REGULAR,
         ],
@@ -549,7 +563,7 @@
         and gate_proj.shape[2] % 128 == 0
         and down_proj.shape[2] % 128 == 0
         and gate_proj.shape[1] % 16 == 0
-        and down_proj.shape[1] % 16 == 0
+        and down_proj.shape[1] % (16 * last_cuts) == 0
         and 2 * group_size * toks == lanes * n_fs
     )
     if whole_tiles:

time: 171 us -> 168 us (0.982)
  Pallas kernels: 170 us -> 168 us
    pallas_call x1, Pallas kernels: 167 us -> 165 us  [shards_fused(): pl.pallas_call(functools.partial(fused_kernel, n_fs, n_tp), out_shape=(pl...]
where the time goes in v4:
time: 168 us
  Pallas kernels  168 us (100%)
    pallas_call x1, Pallas kernels, shards_fused(): pl.pallas_call(functools.partial(fused_kernel, n_fs, n_tp), out_shape=(pl...  165 us

profile of v4, /device:TPU:0, one launch (start us, length us, event | category | flops | bytes accessed | tf_op | source)
XLA Modules:
  0.0 168.3 jit_solution(6358399544951878654)
XLA Ops:
  0.6 164.8 %shard_map.102 = (bf16[2048,512]{1,0:T(8,128)(2,1)S(1)}, bf16[2048,512]{1,0:T(8,128)(2,1)S(1)}, bf16[512,2048]{1,0:T(8,128)(2,1)S(1)}, bf16[128,128]{1,0:T(8,128)(2,1)S(1)}, bf16[4,128,512]{2,1,0:T(8,128)(2,1)S(1)}) custom-call(bf16[128,2048]{1,0:T(8,128)(2,1)} %x_in.1, s32[2,128]{1,0:T(2,128)} %bitcast.6, f32[2,128]{1,0:T(2,128)} %bitcast.7, ...), custom_call_target="tpu_custom_call" | custom-call | tf_op jit(solution)/shard_map/pallas_call | solution.py:490
  165.4 2.9 %shard_map.103 = (bf16[128,2048]{1,0:T(8,128)(2,1)}, bf16[2048,512]{1,0:T(8,128)(2,1)}, bf16[2048,512]{1,0:T(8,128)(2,1)}, bf16[512,2048]{1,0:T(8,128)(2,1)}) custom-call(bf16[128,128]{1,0:T(8,128)(2,1)S(1)} %get-tuple-element.13.perm, bf16[4,128,512]{2,1,0:T(8,128)(2,1)S(1)} %get-tuple-element.14.fin_rx, bf16[2048,512]{1,0:T(8,128)(2,1)S(1)} %get-tuple-element.15.gate, ...), custom_call_target="tpu_custom_call" | custom-call | tf_op jit(solution)/shard_map/pallas_call | solution.py:539

commit v5 on v4

--- a/solution.py
+++ b/solution.py
@@ -81,8 +81,8 @@
     gate_st, up_st, down_st, gate_tx, up_tx, down_tx, early_st, early_tx,
     tok_tx, rows, wt_tx, wt_rx, wcol, hidden, own,
     part_tx, part_rx, sum_tx, sum_rx, fin_tx,
-    in_sem, ld_sem, w_send, w_recv, tok_send, tok_recv, wt_send, wt_recv, ex_send, ex_recv,
-    red_send, red_recv, y_send, y_recv, fin_send, fin_recv, early_sem, met_sem,
+    in_sem, ld_sem, early_sem, met_sem, sent, w_recv, tok_recv, wt_recv, ex_recv, red_recv,
+    y_recv, fin_recv,
 ):
     f32, bf16 = jnp.float32, jnp.bfloat16
     fs, tp = lax.axis_index("fs"), lax.axis_index("tp")
@@ -134,11 +134,13 @@
 
     far, close = targets((outer_far, inner_far)), targets((mate, layer))
     ahead = 1
+    batches = (far[:ahead], close, far[ahead:])
     plan = far[:ahead] + close + far[ahead:]
-
-    def load(m, tgt):
+    first_of = {0: 0, ahead: 1, ahead + len(close): 2}
+
+    def load(m, tgt, batch):
         at = pl.ds(tgt * n_tp, n_tp)
-        return pltpu.make_async_copy(srcs[m].at[at], stages[m].at[at], ld_sem.at[m, tgt])
+        return pltpu.make_async_copy(srcs[m].at[at], stages[m].at[at], ld_sem.at[m, batch])
 
     small = [
         pltpu.make_async_copy(src, dst, in_sem.at[i])
@@ -151,14 +153,14 @@
 
     def load_early(m, j):
         return pltpu.make_async_copy(
-            srcs[m].at[lines[j] * n_tp + tp], early_st.at[m, j], early_sem.at[m, j]
+            srcs[m].at[lines[j] * n_tp + tp], early_st.at[m, j], early_sem
         )
 
     small[0].start()
     for m, j in early:
         load_early(m, j).start()
     for m in (0, 1):
-        load(m, plan[0][0]).start()
+        load(m, plan[0][0], 0).start()
 
     lane_id = lax.broadcasted_iota(jnp.int32, (toks, lanes), 1)
     row_id = lax.broadcasted_iota(jnp.int32, (toks, lanes), 0)
@@ -183,7 +185,6 @@
 
     def cast(ms, tgt):
         for m in ms:
-            load(m, tgt).wait()
 
             @pl.loop(0, n_tp)
             def _(t):
@@ -202,7 +203,7 @@
             for m in (0, 1):
                 pltpu.make_async_remote_copy(
                     src_ref=txs[m].at[tgt * n_tp + to], dst_ref=block_at(m),
-                    send_sem=w_send.at[m], recv_sem=w_recv.at[m],
+                    send_sem=sent, recv_sem=w_recv.at[m],
                     device_id=(tgt, to), device_id_type=MESH,
                 ).start()
         if same:
@@ -211,8 +212,14 @@
                     txs[m].at[fs * n_tp + tp], block_at(m), w_recv.at[m]
                 ).start()
 
+    def loaded(m, batch, count):
+        all_here(stages[m].at[pl.ds(0, count * n_tp)], ld_sem.at[m, batch])
+
     def step_plan(first, last):
         for k in range(first, last):
+            if k in first_of:
+                for m in (0, 1):
+                    loaded(m, first_of[k], len(batches[first_of[k]]))
             if k < len(plan):
                 cast((0, 1), plan[k][0])
             if k > 0:
@@ -233,7 +240,7 @@
                 to = lax.rem(tp + t, n_tp)
                 pltpu.make_async_remote_copy(
                     src_ref=down_tx.at[(tgt * n_tp + to,) + piece_of], dst_ref=land,
-                    send_sem=w_send.at[2 + c], recv_sem=w_recv.at[2 + c],
+                    send_sem=sent, recv_sem=w_recv.at[2 + c],
                     device_id=(tgt, to), device_id_type=MESH,
                 ).start()
             if same:
@@ -241,24 +248,24 @@
                     down_tx.at[(fs * n_tp + tp,) + piece_of], land, w_recv.at[2 + c]
                 ).start()
 
+    all_here(early_st, early_sem)
     for m, j in early:
-        load_early(m, j).wait()
         early_tx[m, j] = (early_st[m, j] * gain).astype(bf16)
     pl.semaphore_wait(barrier, plane + 2)
     greet_plane(met_sem)
     for m, j in early:
         pltpu.make_async_remote_copy(
             src_ref=early_tx.at[m, j], dst_ref=block_at(m),
-            send_sem=w_send.at[m], recv_sem=w_recv.at[m],
+            send_sem=sent, recv_sem=w_recv.at[m],
             device_id=(lines[j], tp), device_id_type=MESH,
         ).start()
     step_plan(0, 1)
     for copy in small[1:]:
         copy.start()
-    for ms in ((0, 1), (2,)):
-        for tgt, _, _ in plan[1:] if ms[0] == 0 else plan:
-            for m in ms:
-                load(m, tgt).start()
+    for m, batch in ((0, 1), (0, 2), (2, 0)):
+        for tgt, _, _ in batches[batch] if m == 0 else plan:
+            for n in (0, 1) if m == 0 else (2,):
+                load(n, tgt, batch).start()
     pl.semaphore_wait(met_sem, plane - 1)
     step_plan(1, ahead + 1)
 
@@ -287,7 +294,7 @@
         tgt = lax.rem(fs + j, n_fs)
         pltpu.make_async_remote_copy(
             src_ref=tok_tx.at[span(tgt)], dst_ref=rows.at[tp, span(fs)],
-            send_sem=tok_send, recv_sem=tok_recv,
+            send_sem=sent, recv_sem=tok_recv,
             device_id=(tgt, tp), device_id_type=MESH,
         ).start()
 
@@ -311,34 +318,35 @@
         tgt = dev // n_tp
         pltpu.make_async_remote_copy(
             src_ref=wt_tx.at[tgt], dst_ref=wt_rx.at[tp, fs],
-            send_sem=wt_send, recv_sem=wt_recv,
+            send_sem=sent, recv_sem=wt_recv,
             device_id=(tgt, lax.rem(dev, n_tp)), device_id_type=MESH,
         ).start()
 
     pltpu.make_async_copy(wt_tx.at[fs], wt_rx.at[tp, fs], wt_recv).start()
 
     step_plan(ahead + 1, len(plan) + 1)
+    loaded(2, 0, len(plan))
     for tgt, _, _ in plan:
         cast((2,), tgt)
     for c in range(len(cuts)):
         send_cut(c)
 
-    def swap(src, dst, to, send_sem, recv_sem):
+    def swap(src, dst, to, recv_sem):
         return pltpu.make_async_remote_copy(
-            src_ref=src, dst_ref=dst, send_sem=send_sem, recv_sem=recv_sem,
+            src_ref=src, dst_ref=dst, send_sem=sent, recv_sem=recv_sem,
             device_id=(fs, to), device_id_type=MESH,
         )
 
     all_here(rows.at[tp], tok_recv)
-    cross = swap(rows.at[tp], rows.at[tp], across, ex_send.at[0], ex_recv.at[0])
+    cross = swap(rows.at[tp], rows.at[tp], across, ex_recv.at[0])
     cross.start()
-    near = swap(rows.at[tp], rows.at[tp], partner, ex_send.at[1], ex_recv.at[1])
+    near = swap(rows.at[tp], rows.at[tp], partner, ex_recv.at[1])
     near.start()
-    cross.wait()
-    other = swap(rows.at[across], rows.at[across], partner, ex_send.at[2], ex_recv.at[2])
+    cross.wait_recv()
+    other = swap(rows.at[across], rows.at[across], partner, ex_recv.at[2])
     other.start()
-    near.wait()
-    other.wait()
+    near.wait_recv()
+    other.wait_recv()
     all_here(wt_rx, wt_recv)
     mine = lax.rem(lane_id, span_lanes) == tp * per + in_group
 
@@ -368,12 +376,12 @@
         return pl.ds(pl.multiple_of(piece(p) * step * per, step * per), step * per)
 
     def reduce_near(k):
-        return swap(part_tx.at[k], part_rx.at[k], partner, red_send.at[k], red_recv.at[k])
+        return swap(part_tx.at[k], part_rx.at[k], partner, red_recv.at[k])
 
     def over(k, p):
         at = piece_rows(p)
         return swap(
-            sum_tx.at[k, at], sum_rx.at[k, at], across, y_send.at[k, p], y_recv.at[k, p]
+            sum_tx.at[k, at], sum_rx.at[k, at], across, y_recv.at[k, p if k == chunks - 1 else min(p, 1)]
         )
 
     def multiply(k):
@@ -392,7 +400,7 @@
         own[k, 1] = partial(pair * 2 + core)
 
     def cross_over(k):
-        reduce_near(k).wait()
+        reduce_near(k).wait_recv()
         for p in range(pieces):
             at = piece_rows(p)
             sum_tx[k, at] = (own[k, 0, at] + part_rx[k, 1 - pair, at].astype(f32)).astype(bf16)
@@ -402,7 +410,11 @@
         for p in ps:
             at = piece_rows(p)
             own_part = own[k, 1, at] + part_rx[k, pair, at].astype(f32)
-            over(k, p).wait()
+            if k == chunks - 1 or p == 0:
+                over(k, p).wait_recv()
+            elif p == 1:
+                rest = sum_rx.at[k, pl.ds(0, toks - step * per)]
+                all_here(rest, y_recv.at[k, 1])
             fin_tx[k, at] = (own_part + sum_rx[k, at].astype(f32)).astype(bf16)
             for i in range(step):
                 to = piece(p) * step + i
@@ -411,7 +423,7 @@
                 def _():
                     pltpu.make_async_remote_copy(
                         src_ref=fin_tx.at[k, span(to)], dst_ref=fin_rx.at[k, span(fs)],
-                        send_sem=fin_send, recv_sem=fin_recv,
+                        send_sem=sent, recv_sem=fin_recv,
                         device_id=(to, tp), device_id_type=MESH,
                     ).start()
 
@@ -441,17 +453,16 @@
     for k in range(1, chunks):
         give_back(k, (1, 2, 3))
 
-    for m in (0, 1):
-        all_sent(txs[m].at[pl.ds(0, n_dev - 1)], w_send.at[m])
-    for c, (_, _, count) in enumerate(cuts):
-        all_sent(
-            down_tx.at[pl.ds(0, n_dev - 1), pl.ds(0, count), pl.ds(0, lanes)], w_send.at[2 + c]
-        )
-    all_sent(tok_tx.at[pl.ds(0, toks - per)], tok_send)
-    all_sent(wt_rx.at[0, pl.ds(0, n_fs - 1)], wt_send)
+    for tx in txs:
+        all_sent(tx.at[pl.ds(0, n_dev - 1)], sent)
+    all_sent(tok_tx.at[pl.ds(0, toks - per)], sent)
+    all_sent(wt_rx.at[0, pl.ds(0, n_fs - 1)], sent)
     for _ in range(n_tp - 1):
-        all_sent(wt_rx.at[0], wt_send)
-    all_sent(fin_tx.at[:, pl.ds(0, toks - per)], fin_send)
+        all_sent(wt_rx.at[0], sent)
+    all_sent(rows.at[pl.ds(0, 3)], sent)
+    all_sent(part_tx, sent)
+    all_sent(sum_tx, sent)
+    all_sent(fin_tx.at[:, pl.ds(0, toks - per)], sent)
     all_here(fin_rx, fin_recv)
 
 
@@ -523,9 +534,9 @@
             pltpu.VMEM((chunks, toks, wide), bf16),
             pltpu.VMEM((chunks, toks, wide), bf16),
             pltpu.VMEM((chunks, toks, wide), bf16),
-            dma((4,)), dma((3, n_fs)), dma((1 + chunks + last_cuts,)), dma((1 + chunks + last_cuts,)), dma, dma, dma, dma,
-            dma((3,)), dma((3,)), dma((chunks,)), dma((chunks,)), dma((chunks, 4)),
-            dma((chunks, 4)), dma, dma, dma((2, 2)), pltpu.SemaphoreType.REGULAR,
+            dma((4,)), dma((3, 3)), dma, pltpu.SemaphoreType.REGULAR, dma,
+            dma((1 + chunks + last_cuts,)), dma, dma, dma((3,)), dma((chunks,)),
+            dma((chunks, 4)), dma,
         ],
         compiler_params=pltpu.CompilerParams(
             collective_id=0, has_side_effects=True, vmem_limit_bytes=47 * 1024 * 1024

time: 168 us -> 168 us (level)
  no operation moved by 1% of the time
where the time goes in v5:
time: 168 us
  Pallas kernels  167 us (99%)
    pallas_call x1, Pallas kernels, shards_fused(): pl.pallas_call(functools.partial(fused_kernel, n_fs, n_tp), out_shape=(pl...  164 us

profile of v5, /device:TPU:0, one launch (start us, length us, event | category | flops | bytes accessed | tf_op | source)
XLA Modules:
  0.0 167.9 jit_solution(2518925792242298686)
XLA Ops:
  0.6 164.4 %shard_map.102 = (bf16[2048,512]{1,0:T(8,128)(2,1)S(1)}, bf16[2048,512]{1,0:T(8,128)(2,1)S(1)}, bf16[512,2048]{1,0:T(8,128)(2,1)S(1)}, bf16[128,128]{1,0:T(8,128)(2,1)S(1)}, bf16[4,128,512]{2,1,0:T(8,128)(2,1)S(1)}) custom-call(bf16[128,2048]{1,0:T(8,128)(2,1)} %x_in.1, s32[2,128]{1,0:T(2,128)} %bitcast.6, f32[2,128]{1,0:T(2,128)} %bitcast.7, ...), custom_call_target="tpu_custom_call" | custom-call | tf_op jit(solution)/shard_map/pallas_call | solution.py:501
  165.1 2.9 %shard_map.103 = (bf16[128,2048]{1,0:T(8,128)(2,1)}, bf16[2048,512]{1,0:T(8,128)(2,1)}, bf16[2048,512]{1,0:T(8,128)(2,1)}, bf16[512,2048]{1,0:T(8,128)(2,1)}) custom-call(bf16[128,128]{1,0:T(8,128)(2,1)S(1)} %get-tuple-element.13.perm, bf16[4,128,512]{2,1,0:T(8,128)(2,1)S(1)} %get-tuple-element.14.fin_rx, bf16[2048,512]{1,0:T(8,128)(2,1)S(1)} %get-tuple-element.15.gate, ...), custom_call_target="tpu_custom_call" | custom-call | tf_op jit(solution)/shard_map/pallas_call | solution.py:550
